TPU v7x, 32 devices: a whole 2x2x4 slice. The times are simulated.
32 devices in a mesh: ra: 8 (over z, y), cb: 4 (over x, core).
Axes of the slice: x: 2, y: 2, z: 4, core: 2. Of those that a mesh axis runs over, the one named last changes fastest.
Arguments:
- activations: bfloat16 [512, 4224], P('cb', 'ra'), may hold values from -160 to 160, as said below
- norm_gain: float32 [2, 4224], replicated, may hold values from 0.1 to 1.9
- gate_weight: float32 [2, 4224, 11520], P(None, None, 'ra'), may hold values from -0.09375 to 0.09375
- gate_scale: float32 [2, 11520], P(None, 'ra'), may hold values from 0.3 to 3
- value_weight: float32 [2, 4224, 11520], P(None, None, 'ra'), may hold values from -0.09375 to 0.09375
- value_scale: float32 [2, 11520], P(None, 'ra'), may hold values from 0.3 to 3
- gate_taps: float32 [2, 3, 11520], P(None, None, 'ra'), may hold values from -3 to 3
- value_taps: float32 [2, 3, 11520], P(None, None, 'ra'), may hold values from -3 to 3
- down_weight: float32 [2, 11520, 4224], P(None, None, 'ra'), may hold values from -0.0546875 to 0.0546875
- down_scale: float32 [2, 4224], P(None, 'ra'), may hold values from 0.3 to 3
- final_gain: float32 [4224], P('ra'), may hold values from 0.1 to 1.9
Outputs:
- normalized: bfloat16 [512, 4224], P('cb', 'ra')
Inputs may be any that keep to these rules, and one draw needn't show every extreme that they name: `activations`: rows and columns have unequal scales.
All inputs are finite; a program needn't handle non-finite values.
Results may differ from a plain program's by a relative error of at most 0.017.
Values may be sent and summed in bfloat16 or wider, within the bound.
A program may use at most 320 MiB of HBM per device.

v0:
```python
import jax
import jax.numpy as jnp
from jax import lax
from jax.sharding import PartitionSpec as P

D = 4224


epsilon = 1e-06
resid_scale = 0.5


def from_behind(value, axis, by):
    length = lax.axis_size(axis)
    pairs = [(i, i + by) for i in range(length) if 0 <= i + by < length]
    return lax.ppermute(value, axis, pairs)


def conv_local(values_in, earlier, tap_weights):
    seq_len = values_in.shape[0]
    taps = tap_weights.shape[0]
    padded = jnp.concatenate([earlier, values_in], axis=0)
    total = jnp.zeros(values_in.shape, jnp.float32)
    for offset in range(taps):
        total = total + tap_weights[offset] * padded[offset : offset + seq_len]
    return total


def per_device(
    activations,
    norm_gain,
    gate_weight,
    gate_scale,
    value_weight,
    value_scale,
    gate_taps,
    value_taps,
    down_weight,
    down_scale,
    final_gain,
):
    row_count, width_part = activations.shape
    tok_rows = activations
    layer_count = gate_weight.shape[0]
    taps = gate_taps.shape[1]
    for layer_idx in range(layer_count):
        wide_rows = tok_rows.astype(jnp.float32)
        full_rows = lax.all_gather(tok_rows, "ra", axis=1, tiled=True).astype(jnp.float32)
        inv_norm = lax.rsqrt(jnp.mean(full_rows * full_rows, axis=1, keepdims=True) + epsilon)
        scaled = (full_rows * norm_gain[layer_idx]).astype(jnp.bfloat16)
        gate_pre = (
            jnp.dot(
                scaled,
                gate_weight[layer_idx].astype(jnp.bfloat16),
                preferred_element_type=jnp.float32,
            )
            * inv_norm
            * gate_scale[layer_idx]
        )
        value_pre = (
            jnp.dot(
                scaled,
                value_weight[layer_idx].astype(jnp.bfloat16),
                preferred_element_type=jnp.float32,
            )
            * inv_norm
            * value_scale[layer_idx]
        )
        gate_prev, value_prev = from_behind(
            (gate_pre[row_count - taps + 1 :], value_pre[row_count - taps + 1 :]), "cb", 1
        )
        gate_conv = conv_local(gate_pre, gate_prev, gate_taps[layer_idx])
        value_conv = conv_local(value_pre, value_prev, value_taps[layer_idx])
        down_bf = down_weight[layer_idx].astype(jnp.bfloat16)
        hidden = (jax.nn.silu(gate_conv) * value_conv).astype(jnp.bfloat16)
        down = jnp.dot(
            lax.all_gather(hidden, "ra", axis=1, tiled=True),
            down_bf,
            preferred_element_type=jnp.float32,
        )
        tok_rows = (resid_scale * wide_rows + down * down_scale[layer_idx]).astype(jnp.bfloat16)
    wide_rows = tok_rows.astype(jnp.float32)
    sq_final = lax.psum(jnp.sum(wide_rows * wide_rows, axis=1), "ra")
    inv_norm = lax.rsqrt(sq_final[:, None] / D + epsilon)
    return (wide_rows * inv_norm * final_gain).astype(jnp.bfloat16)


def solution(mesh):
    in_specs = (
        P("cb", "ra"),
        P(),
        P(None, None, "ra"),
        P(None, "ra"),
        P(None, None, "ra"),
        P(None, "ra"),
        P(None, None, "ra"),
        P(None, None, "ra"),
        P(None, None, "ra"),
        P(None, "ra"),
        P("ra"),
    )
    out_specs = P("cb", "ra")
    return jax.shard_map(
        per_device, mesh=mesh, in_specs=in_specs, out_specs=out_specs, check_vma=False
    )
```

profile of v0, /device:TPU:0, one launch (start us, length us, event | category | flops | bytes accessed | tf_op | source)
XLA Modules:
  0.0 316.4 jit_solution(9558296523419066182)
XLA Ops:
  6.5 0.7 all-gather.5.cloned.1.call-update
  7.3 24.9 %convert.12 = bf16[2,4224,1440]{1,2,0:T(8,128)(2,1)} convert(f32[2,4224,1440]{1,2,0:T(8,128)} %param.13) | non-fusion elementwise | flops 12165120 | bytes 72990720 | tf_op jit(solution)/shard_map/convert.5
  32.2 24.9 %convert.13 = bf16[2,4224,1440]{1,2,0:T(8,128)(2,1)} convert(f32[2,4224,1440]{1,2,0:T(8,128)} %param.15) | non-fusion elementwise | flops 12165120 | bytes 72990720 | tf_op jit(solution)/shard_map/convert.4
  57.3 1.8 fusion.15
  59.1 8.2 %fusion.13 = f32[128,1440]{0,1:T(8,128)S(1)} fusion(bf16[2,4224,1440]{1,2,0:T(8,128)(2,1)} %convert.12, bf16[128,4224]{0,1:T(8,128)(2,1)} %all-gather.5.cloned.1.call-done, f32[4224]{0:T(1024)S(1)} %get-tuple-element.18, f32[1440]{0:T(1024)S(1)} %get-tuple-element.20, f32[128]{0:T(128)S(1)} %add_rsqrt_fusion.2), kind=kOutput, calls=%fused_computation.23 | convolution fusion | flops 1559126016 | bytes 14006912 | tf_op jit(solution)/shard_map/dot_general | solution.py:52
  67.6 0.3 copy.12
  67.9 2.4 collective-permute-start
  70.3 8.0 %fusion.12 = f32[128,1440]{0,1:T(8,128)S(1)} fusion(bf16[2,4224,1440]{1,2,0:T(8,128)(2,1)} %convert.13, bf16[128,4224]{0,1:T(8,128)(2,1)S(1)} %copy-done, f32[4224]{0:T(1024)S(1)} %get-tuple-element.18, f32[1440]{0:T(1024)S(1)} %get-tuple-element.22, f32[128]{0:T(128)S(1)} %add_rsqrt_fusion.2), kind=kOutput, calls=%fused_computation.22 | convolution fusion | flops 1559126016 | bytes 14006912 | tf_op jit(solution)/shard_map/dot_general | solution.py:61
  78.5 0.3 copy.14
  78.8 4.5 %collective-permute-start.1 = (f32[2,1440]{1,0:T(2,128)S(1)}, f32[2,1440]{1,0:T(2,128)S(1)}, u32[]{:S(2)}, u32[]{:S(2)}) collective-permute-start(f32[2,1440]{1,0:T(2,128)S(1)} %copy.14), channel_id=1, source_target_pairs={{0,1},{1,2},{2,3},{4,5},{5,6},{6,7},{8,9},{9,10},{10,11},{12,13},{... | collective-permute-start | bytes 34568 | tf_op jit(solution)/shard_map/ppermute | solution.py:16
  83.5 0.3 copy.13
  83.8 0.3 collective-permute-done.1
  84.1 0.3 copy.15
  84.4 3.3 %fusion.40 = bf16[128,1440]{0,1:T(8,128)(2,1)} fusion(f32[2,1440]{0,1:T(8,128)S(1)} %copy.15, f32[128,1440]{0,1:T(8,128)S(1)} %fusion.12, f32[128,1440]{0,1:T(8,128)S(1)} %fusion.13, f32[2,1440]{0,1:T(8,128)S(1)} %copy.13, f32[1440]{0:T(1024)S(1)} %get-tuple-element.12, f32[1440]{0:T(1024)S(1)} %get-tuple-element.13, f32[1440]{0:T(1024)S(1)} %get-tuple-element.14, ...), kind=kLoop, calls=%fused_computation.58 | loop fusion | flops 3686400 | bytes 1900800 | tf_op jit(solution)/shard_map/convert_element_type | solution.py:75
  87.8 25.0 %convert.14 = bf16[2,11520,528]{1,2,0:T(8,128)(2,1)} convert(f32[2,11520,528]{1,2,0:T(8,128)} %param.19) | non-fusion elementwise | flops 12165120 | bytes 72990720 | tf_op jit(solution)/shard_map/convert.3
  112.8 34.9 %all-gather.7.cloned.1.call-done = bf16[128,11520]{0,1:T(8,128)(2,1)} async-done(((bf16[128,1440]{0,1:T(8,128)(2,1)}), bf16[128,11520]{0,1:T(8,128)(2,1)}) %all-gather.7.cloned.1.call-update) | async-done | bytes 2949136 | tf_op jit(solution)/shard_map/all_gather | solution.py:77
  147.7 9.3 %fusion.24 = bf16[128,528]{0,1:T(8,128)(2,1)} fusion(bf16[128,11520]{0,1:T(8,128)(2,1)} %all-gather.7.cloned.1.call-done, bf16[2,11520,528]{1,2,0:T(8,128)(2,1)} %convert.14, bf16[128,528]{0,1:T(8,128)(2,1)S(1)} %copy-done.2, f32[528]{0:T(1024)S(1)} %get-tuple-element.24), kind=kOutput, calls=%fused_computation.42 | convolution fusion | flops 1557473280 | bytes 15386688 | tf_op jit(solution)/shard_map/dot_general | solution.py:76
  157.2 39.1 %all-gather.9.cloned.1.call-done = bf16[128,4224]{0,1:T(8,128)(2,1)} async-done(((bf16[128,528]{0,1:T(8,128)(2,1)}), bf16[128,4224]{0,1:T(8,128)(2,1)}) %all-gather.9.cloned.1.call-update) | async-done | bytes 1081360 | tf_op jit(solution)/shard_map/all_gather | solution.py:48
  196.3 1.8 fusion.17
  198.1 8.2 %fusion.11 = f32[128,1440]{0,1:T(8,128)S(1)} fusion(bf16[2,4224,1440]{1,2,0:T(8,128)(2,1)} %convert.12, bf16[128,4224]{0,1:T(8,128)(2,1)} %all-gather.9.cloned.1.call-done, f32[4224]{0:T(1024)S(1)} %get-tuple-element.17, f32[1440]{0:T(1024)S(1)} %get-tuple-element.19, f32[128]{0:T(128)S(1)} %add_rsqrt_fusion.1), kind=kOutput, calls=%fused_computation.21 | convolution fusion | flops 1559126016 | bytes 14006912 | tf_op jit(solution)/shard_map/dot_general | solution.py:52
  206.9 1.3 collective-permute-start.2
  208.2 8.0 %fusion.10 = f32[128,1440]{0,1:T(8,128)S(1)} fusion(bf16[2,4224,1440]{1,2,0:T(8,128)(2,1)} %convert.13, bf16[128,4224]{0,1:T(8,128)(2,1)S(1)} %copy-done.1, f32[4224]{0:T(1024)S(1)} %get-tuple-element.17, f32[1440]{0:T(1024)S(1)} %get-tuple-element.21, f32[128]{0:T(128)S(1)} %add_rsqrt_fusion.1), kind=kOutput, calls=%fused_computation.20 | convolution fusion | flops 1559126016 | bytes 14006912 | tf_op jit(solution)/shard_map/dot_general | solution.py:61
  216.4 0.3 copy.18
  216.7 4.1 %collective-permute-start.3 = (f32[2,1440]{1,0:T(2,128)S(1)}, f32[2,1440]{1,0:T(2,128)S(1)}, u32[]{:S(2)}, u32[]{:S(2)}) collective-permute-start(f32[2,1440]{1,0:T(2,128)S(1)} %copy.18), channel_id=1, source_target_pairs={{0,1},{1,2},{2,3},{4,5},{5,6},{6,7},{8,9},{9,10},{10,11},{12,13},{... | collective-permute-start | bytes 34568 | tf_op jit(solution)/shard_map/ppermute | solution.py:16
  220.8 0.3 copy.17
  221.1 0.5 collective-permute-done.3
  221.6 0.3 copy.19
  221.9 3.3 %fusion.30 = bf16[128,1440]{0,1:T(8,128)(2,1)} fusion(f32[2,1440]{0,1:T(8,128)S(1)} %copy.19, f32[128,1440]{0,1:T(8,128)S(1)} %fusion.10, f32[128,1440]{0,1:T(8,128)S(1)} %fusion.11, f32[2,1440]{0,1:T(8,128)S(1)} %copy.17, f32[1440]{0:T(1024)S(1)} %get-tuple-element.15, f32[1440]{0:T(1024)S(1)} %get-tuple-element.16, f32[1440]{0:T(1024)S(1)} %get-tuple-element.11, ...), kind=kLoop, calls=%fused_computation.48 | loop fusion | flops 3686400 | bytes 1900800 | tf_op jit(solution)/shard_map/convert_element_type | solution.py:75
  225.2 57.5 %all-gather.11.cloned.1.call-done = bf16[128,11520]{0,1:T(8,128)(2,1)} async-done(((bf16[128,1440]{0,1:T(8,128)(2,1)}), bf16[128,11520]{0,1:T(8,128)(2,1)}) %all-gather.11.cloned.1.call-update) | async-done | bytes 2949136 | tf_op jit(solution)/shard_map/all_gather | solution.py:77
  282.7 7.2 %multiply_reduce_fusion = (f32[128]{0:T(128)S(1)}, f32[128,528]{0,1:T(8,128)S(1)}) fusion(f32[528]{0:T(1024)S(1)} %get-tuple-element.23, bf16[128,11520]{0,1:T(8,128)(2,1)} %all-gather.11.cloned.1.call-done, bf16[2,11520,528]{1,2,0:T(8,128)(2,1)} %convert.14, bf16[128,528]{0,1:T(8,128)(2,1)S(1)} %copy-done.3), kind=kOutput, calls=%fused_computation.72 | convolution fusion | flops 1557675904 | bytes 15522368 | tf_op jit(solution)/shard_map/dot_general | solution.py:76
  290.0 19.1 %psum.7 = f32[128]{0:T(128)S(1)} all-reduce(f32[128]{0:T(128)S(1)} %get-tuple-element.25), channel_id=1, replica_groups=mesh['ra'=8,'cb'=4] {'ra'}, use_global_device_ids=true, to_apply=%region_3.4 | all-reduce | flops 128 | bytes 1024 | tf_op jit(solution)/shard_map/psum | solution.py:83
  309.0 0.8 multiply_convert_fusion
  (45 shorter events, 2.1 us)
Async XLA Ops:
  6.5 50.7 %all-gather.5.cloned.1.call-start = ((), (), s32[]{:S(2)}) async-start(), calls=%async_computation | async-start | bytes 1216512 | tf_op jit(solution)/shard_map/all_gather | solution.py:48
  7.3 140.5 %all-gather.7.cloned.1.call-start = ((), (), s32[]{:S(2)}) async-start(), calls=%async_computation.1 | async-start | bytes 3317760 | tf_op jit(solution)/shard_map/all_gather | solution.py:77
  32.2 24.9 %copy-start.7 = (f32[2,1440]{1,0:T(2,128)S(1)}, f32[2,1440]{1,0:T(2,128)}, u32[]{:S(2)}) copy-start(f32[2,1440]{1,0:T(2,128)} %param.14) | copy-start | bytes 34564
  32.2 24.9 %copy-start.8 = (f32[2,1440]{1,0:T(2,128)S(1)}, f32[2,1440]{1,0:T(2,128)}, u32[]{:S(2)}) copy-start(f32[2,1440]{1,0:T(2,128)} %param.16) | copy-start | bytes 34564
  32.2 25.0 %copy-start.6 = (f32[2,4224]{1,0:T(2,128)S(1)}, f32[2,4224]{1,0:T(2,128)}, u32[]{:S(2)}) copy-start(f32[2,4224]{1,0:T(2,128)} %param.12) | copy-start | bytes 101380
  67.3 2.9 copy-start
  67.9 15.6 %collective-permute-start = (f32[2,1440]{1,0:T(2,128)S(1)}, f32[2,1440]{1,0:T(2,128)S(1)}, u32[]{:S(2)}, u32[]{:S(2)}) collective-permute-start(f32[2,1440]{1,0:T(2,128)S(1)} %copy.12), channel_id=1, source_target_pairs={{0,1},{1,2},{2,3},{4,5},{5,6},{6,7},{8,9},{9,10},{10,11},{12,13},{... | collective-permute-start | bytes 34568 | tf_op jit(solution)/shard_map/ppermute | solution.py:16
  78.3 5.0 %copy-start.4 = (f32[2,3,1440]{2,0,1:T(2,128)S(1)}, f32[2,3,1440]{2,0,1:T(2,128)}, u32[]{:S(2)}) copy-start(f32[2,3,1440]{2,0,1:T(2,128)} %param.18) | copy-start | bytes 103684
  78.3 5.0 %copy-start.5 = (f32[2,3,1440]{2,0,1:T(2,128)S(1)}, f32[2,3,1440]{2,0,1:T(2,128)}, u32[]{:S(2)}) copy-start(f32[2,3,1440]{2,0,1:T(2,128)} %param.17) | copy-start | bytes 103684
  78.8 5.3 %collective-permute-start.1 = (f32[2,1440]{1,0:T(2,128)S(1)}, f32[2,1440]{1,0:T(2,128)S(1)}, u32[]{:S(2)}, u32[]{:S(2)}) collective-permute-start(f32[2,1440]{1,0:T(2,128)S(1)} %copy.14), channel_id=1, source_target_pairs={{0,1},{1,2},{2,3},{4,5},{5,6},{6,7},{8,9},{9,10},{10,11},{12,13},{... | collective-permute-start | bytes 34568 | tf_op jit(solution)/shard_map/ppermute | solution.py:16
  87.7 25.1 %copy-start.9 = (f32[2,528]{1,0:T(2,128)S(1)}, f32[2,528]{1,0:T(2,128)}, u32[]{:S(2)}) copy-start(f32[2,528]{1,0:T(2,128)} %param.20) | copy-start | bytes 12676
  87.7 60.0 %copy-start.2 = (bf16[128,528]{0,1:T(8,128)(2,1)S(1)}, bf16[128,528]{0,1:T(8,128)(2,1)}, u32[]{:S(2)}) copy-start(bf16[128,528]{0,1:T(8,128)(2,1)} %param.11) | copy-start | bytes 405508
  87.7 108.6 %all-gather.9.cloned.1.call-start = ((), (), s32[]{:S(2)}) async-start(), calls=%async_computation.2 | async-start | bytes 1216512 | tf_op jit(solution)/shard_map/all_gather | solution.py:48
  157.0 125.7 %all-gather.11.cloned.1.call-start = ((), (), s32[]{:S(2)}) async-start(), calls=%async_computation.3 | async-start | bytes 3317760 | tf_op jit(solution)/shard_map/all_gather | solution.py:77
  206.4 1.8 copy-start.1
  206.9 13.9 %collective-permute-start.2 = (f32[2,1440]{1,0:T(2,128)S(1)}, f32[2,1440]{1,0:T(2,128)S(1)}, u32[]{:S(2)}, u32[]{:S(2)}) collective-permute-start(f32[2,1440]{1,0:T(2,128)S(1)} %copy.16), channel_id=1, source_target_pairs={{0,1},{1,2},{2,3},{4,5},{5,6},{6,7},{8,9},{9,10},{10,11},{12,13},{... | collective-permute-start | bytes 34568 | tf_op jit(solution)/shard_map/ppermute | solution.py:16
  216.7 4.9 %collective-permute-start.3 = (f32[2,1440]{1,0:T(2,128)S(1)}, f32[2,1440]{1,0:T(2,128)S(1)}, u32[]{:S(2)}, u32[]{:S(2)}) collective-permute-start(f32[2,1440]{1,0:T(2,128)S(1)} %copy.18), channel_id=1, source_target_pairs={{0,1},{1,2},{2,3},{4,5},{5,6},{6,7},{8,9},{9,10},{10,11},{12,13},{... | collective-permute-start | bytes 34568 | tf_op jit(solution)/shard_map/ppermute | solution.py:16
  221.1 61.6 %copy-start.3 = (bf16[128,528]{0,1:T(8,128)(2,1)S(1)}, bf16[128,528]{0,1:T(8,128)(2,1)}, u32[]{:S(2)}) copy-start(bf16[128,528]{0,1:T(8,128)(2,1)} %fusion.24) | copy-start | bytes 405508
  282.7 26.3 %copy-start.10 = (f32[528]{0:T(1024)S(1)}, f32[528]{0:T(1024)}, u32[]{:S(2)}) copy-start(f32[528]{0:T(1024)} %param.21) | copy-start | bytes 6340
Sparse Core Ops, SparseCore 0:
  9.5 43.2 all-gather.4
  87.8 59.8 all-gather.6
  157.1 39.1 all-gather.8
  225.4 57.3 all-gather.10
where the time goes:
time: 317 us; the launch traced here: 316 us
  waiting for transfers between devices  133 us (42%)
  other arithmetic  85.8 us (27%)
  matrix products  48.9 us (15%)
  blocking collectives  19.1 us (6%)
  between operations  13.4 us (4%)
  starting transfers between devices  12.6 us (4%)
  local copies, waits for them, and re-layouts  3.63 us (1%)
    all_gather x2, waiting for transfers between devices, per_device(): lax.all_gather(hidden, 'ra', axis=1, tiled=True)  92.4 us
    another operation x3, other arithmetic  74.7 us
    all_gather x2, waiting for transfers between devices, per_device(): lax.all_gather(tok_rows, 'ra', axis=1, tiled=True).astype(jnp.float32)  39.1 us
    psum x1, blocking collectives, per_device(): sq_final = lax.psum(jnp.sum(wide_rows * wide_rows, axis=1), 'ra')  19.1 us
    dot_general x2, matrix products, per_device(): jnp.dot(scaled, gate_weight[layer_idx].astype(jnp.bfloat16), preferred_el...  16.5 us
    dot_general x2, matrix products, per_device(): jnp.dot(lax.all_gather(hidden, 'ra', axis=1, tiled=True), down_bf, prefer...  16.4 us
    dot_general x2, matrix products, per_device(): jnp.dot(scaled, value_weight[layer_idx].astype(jnp.bfloat16), preferred_e...  16 us
    ppermute x4, starting transfers between devices, from_behind(): return lax.ppermute(value, axis, pairs)  12.2 us
  transfers between devices with their start and end apart: 8, of which 5 were waited for; matrix products, arithmetic and copies ran while one was open for 29% of the time, Pallas kernels for 0%

commit v1 on v0

--- a/solution.py
+++ b/solution.py
@@ -1,6 +1,10 @@
+import functools
+
 import jax
 import jax.numpy as jnp
 from jax import lax
+from jax.experimental import pallas as pl
+from jax.experimental.pallas import tpu as pltpu
 from jax.sharding import PartitionSpec as P
 
 D = 4224
@@ -26,7 +30,7 @@
     return total
 
 
-def per_device(
+def plain_device(
     activations,
     norm_gain,
     gate_weight,
@@ -85,6 +89,429 @@
     return (wide_rows * inv_norm * final_gain).astype(jnp.bfloat16)
 
 
+MESH = pl.DeviceIdType.MESH
+PIECES = 3
+TILES = 6
+GV_SLOTS = 3
+DOWN_BLOCKS = 10
+DOWN_SLOTS = 6
+
+
+def fused_kernel(
+    n,
+    cols,
+    x_ref,
+    gain_ref,
+    par_ref,
+    dscale_ref,
+    fgain_ref,
+    wg_hbm,
+    wv_hbm,
+    wd_hbm,
+    out_ref,
+    xr,
+    halo,
+    xs,
+    hid,
+    gbuf,
+    vbuf,
+    dbuf,
+    acc,
+    ssq,
+    red,
+    gsem,
+    vsem,
+    dsem,
+    xsend,
+    xrecv,
+    bsend,
+    brecv,
+    hsend,
+    hrecv,
+    rsend,
+    rrecv,
+):
+    layers, units, depth = wg_hbm.shape
+    width, toks = x_ref.shape
+    half = n // 2
+    piece = width // PIECES
+    tile = units // TILES
+    kblock = wd_hbm.shape[2] // DOWN_BLOCKS
+    me = lax.axis_index("ra")
+    col = lax.axis_index("cb")
+    pos = (1 - me % 2) * (me // 2) + (me % 2) * (n - 1 - me // 2)
+
+    def member(p):
+        p = (p + n) % n
+        b = p // half
+        return (1 - b) * (2 * p) + b * (2 * (n - 1 - p) + 1)
+
+    ahead = (member(pos + 1), member(pos - 1))
+
+    def origin(d, h):
+        return member(pos - h) if d == 0 else member(pos + h)
+
+    def gv_copies(g):
+        l, t, slot = g // TILES, g % TILES, g % GV_SLOTS
+        rows = pl.ds(pl.multiple_of(t * tile, 8), tile)
+        return (
+            pltpu.make_async_copy(wg_hbm.at[l, rows], gbuf.at[slot], gsem.at[slot]),
+            pltpu.make_async_copy(wv_hbm.at[l, rows], vbuf.at[slot], vsem.at[slot]),
+        )
+
+    def down_copy(g):
+        l, k, slot = g // DOWN_BLOCKS, g % DOWN_BLOCKS, g % DOWN_SLOTS
+        lanes = pl.ds(pl.multiple_of(k * kblock, 128), kblock)
+        return pltpu.make_async_copy(wd_hbm.at[l, :, lanes], dbuf.at[slot], dsem.at[slot])
+
+    def x_rows(owner, s):
+        return pl.ds(pl.multiple_of(owner * width + s * piece, 16), piece)
+
+    def x_copy(l, d, h, s, sending):
+        rows = x_rows(origin(d, h - sending), s)
+        return pltpu.make_async_remote_copy(
+            src_ref=xr.at[l, rows],
+            dst_ref=xr.at[l, rows],
+            send_sem=xsend.at[l, d, h - 1, s],
+            recv_sem=xrecv.at[l, d, h - 1, s],
+            device_id={"ra": ahead[d]},
+            device_id_type=MESH,
+        )
+
+    def b_copy(l, d, h, s):
+        rows = x_rows(origin(d, h), s)
+        return pltpu.make_async_remote_copy(
+            src_ref=xr.at[l, rows],
+            dst_ref=halo.at[l, rows],
+            send_sem=bsend.at[l, d, h, s],
+            recv_sem=brecv.at[l, d, h, s],
+            device_id={"cb": (col + 1) % cols},
+            device_id_type=MESH,
+        )
+
+    def h_copy(l, d, h, t, sending):
+        rows = pl.ds(pl.multiple_of(origin(d, h - sending) * units + t * tile, 16), tile)
+        return pltpu.make_async_remote_copy(
+            src_ref=hid.at[l, rows],
+            dst_ref=hid.at[l, rows],
+            send_sem=hsend.at[l, d, h - 1, t],
+            recv_sem=hrecv.at[l, d, h - 1, t],
+            device_id={"ra": ahead[d]},
+            device_id_type=MESH,
+        )
+
+    def red_copy(j, owner):
+        return pltpu.make_async_remote_copy(
+            src_ref=red.at[owner],
+            dst_ref=red.at[owner],
+            send_sem=rsend.at[j],
+            recv_sem=rrecv.at[j],
+            device_id={"ra": (me + j) % n},
+            device_id_type=MESH,
+        )
+
+    for g in range(GV_SLOTS):
+        for c in gv_copies(g):
+            c.start()
+    for g in range(DOWN_SLOTS):
+        down_copy(g).start()
+
+    barrier = pltpu.get_barrier_semaphore()
+    for j in range(1, n):
+        pl.semaphore_signal(
+            barrier, inc=1, device_id={"ra": (me + j) % n}, device_id_type=MESH
+        )
+
+    for by in (1, cols - 1):
+        pl.semaphore_signal(
+            barrier, inc=1, device_id={"cb": (col + by) % cols}, device_id_type=MESH
+        )
+
+    mine = pl.ds(pl.multiple_of(me * width, 16), width)
+    xr[0, mine, :] = x_ref[...]
+
+    @pl.when(col == 0)
+    def _():
+        halo[...] = jnp.zeros_like(halo)
+
+    pl.semaphore_wait(barrier, n + 1)
+
+    arrivals = []
+    for h in range(1, half + 1):
+        for s in range(PIECES):
+            for d in range(2):
+                if h < half or s % 2 == d:
+                    arrivals.append((d, h, s))
+    everything = [(0, 0, s) for s in range(PIECES)] + arrivals
+
+    def absorb(l, d, h, s, part):
+        rows = x_rows(origin(d, h), s)
+        wide = (halo if part else xr)[l, rows, :].astype(jnp.float32)
+        lanes = slice(part * toks, (part + 1) * toks)
+        xs[rows, lanes] = (wide * gain_ref[l, rows, :]).astype(jnp.bfloat16)
+        ssq[:, lanes] = ssq[:, lanes] + jnp.sum(wide * wide, axis=0, keepdims=True)
+
+    def absorb_halo(l, d, h, s):
+        @pl.when(col > 0)
+        def _():
+            b_copy(l, d, h, s).wait_recv()
+
+        absorb(l, d, h, s, 1)
+
+    def send_halo(l, d, h, s):
+        @pl.when(col < cols - 1)
+        def _():
+            b_copy(l, d, h, s).start()
+
+    def layer(l, carry):
+        for s in range(PIECES):
+            for d in range(2):
+                x_copy(l, d, 1, s, 1).start()
+        for s in range(PIECES):
+            send_halo(l, 0, 0, s)
+        ssq[...] = jnp.zeros_like(ssq)
+        for s in range(PIECES):
+            absorb(l, 0, 0, s, 0)
+        lag = 4
+        for i, (d, h, s) in enumerate(arrivals):
+            x_copy(l, d, h, s, 0).wait_recv()
+            if h + 1 < half or (h + 1 == half and s % 2 == d):
+                x_copy(l, d, h + 1, s, 1).start()
+            send_halo(l, d, h, s)
+            absorb(l, d, h, s, 0)
+            if i >= lag:
+                absorb_halo(l, *everything[i - lag])
+        for i in range(len(arrivals) - lag, len(everything)):
+            absorb_halo(l, *everything[i])
+
+        inv = lax.rsqrt(ssq[...] / depth + epsilon)
+
+        def tail(value, tap, rows):
+            prev, own = value[:, :toks], value[:, toks:]
+            lane = lax.broadcasted_iota(jnp.int32, own.shape, 1)
+            total = par_ref[l, rows, tap + 2 : tap + 3] * own
+            for by in (1, 2):
+                moved = jnp.where(
+                    lane < by, pltpu.roll(prev, by, 1), pltpu.roll(own, by, 1)
+                )
+                total = total + par_ref[l, rows, tap + 2 - by : tap + 3 - by] * moved
+            return total
+
+        def step(i, carry):
+            @pl.when(i < TILES)
+            def _():
+                g = l * TILES + i
+                slot = g % GV_SLOTS
+                rows = pl.ds(pl.multiple_of(i * tile, 8), tile)
+                for c in gv_copies(g):
+                    c.wait()
+                gate = jnp.dot(
+                    gbuf[slot].astype(jnp.bfloat16), xs[...], preferred_element_type=jnp.float32
+                )
+                gate = gate * inv * par_ref[l, rows, 0:1]
+                gate_conv = tail(jnp.concatenate([gate[:, toks:], gate[:, :toks]], 1), 2, rows)
+                value = jnp.dot(
+                    vbuf[slot].astype(jnp.bfloat16), xs[...], preferred_element_type=jnp.float32
+                )
+                value = value * inv * par_ref[l, rows, 1:2]
+                value_conv = tail(jnp.concatenate([value[:, toks:], value[:, :toks]], 1), 5, rows)
+                hidden = gate_conv / (1.0 + jnp.exp(-gate_conv)) * value_conv
+                place = pl.ds(pl.multiple_of(me * units + i * tile, 16), tile)
+                hid[l, place, :] = hidden.astype(jnp.bfloat16)
+                for d in range(2):
+                    h_copy(l, d, 1, i, 1).start()
+
+                @pl.when(g + GV_SLOTS < layers * TILES)
+                def _():
+                    for c in gv_copies(g + GV_SLOTS):
+                        c.start()
+
+            for h in range(1, half + 1):
+                t = i - h
+                inside = (t >= 0) & (t < TILES)
+                for d in range(2):
+                    even = inside & (t % 2 == d)
+
+                    @pl.when(inside if h < half else even)
+                    def _():
+                        h_copy(l, d, h, t, 0).wait_recv()
+
+                    if h < half:
+
+                        @pl.when(inside if h + 1 < half else even)
+                        def _():
+                            h_copy(l, d, h + 1, t, 1).start()
+
+            return carry
+
+        lax.fori_loop(0, TILES + half, step, 0)
+
+        acc[...] = jnp.zeros_like(acc)
+
+        def down_step(k, carry):
+            g = l * DOWN_BLOCKS + k
+            slot = g % DOWN_SLOTS
+            down_copy(g).wait()
+            rows = pl.ds(pl.multiple_of(k * kblock, 128), kblock)
+            acc[...] += jnp.dot(
+                dbuf[slot].astype(jnp.bfloat16),
+                hid[l, rows, :],
+                preferred_element_type=jnp.float32,
+            )
+
+            @pl.when(g + DOWN_SLOTS < layers * DOWN_BLOCKS)
+            def _():
+                down_copy(g + DOWN_SLOTS).start()
+
+            return carry
+
+        lax.fori_loop(0, DOWN_BLOCKS, down_step, 0)
+        wide = xr[l, mine, :].astype(jnp.float32)
+        xr[l + 1, mine, :] = (resid_scale * wide + acc[...] * dscale_ref[l]).astype(jnp.bfloat16)
+        return carry
+
+    lax.fori_loop(0, layers, layer, 0)
+
+    wide = xr[layers, mine, :].astype(jnp.float32)
+    red[me] = jnp.broadcast_to(jnp.sum(wide * wide, axis=0, keepdims=True), red.shape[1:])
+    for j in range(1, n):
+        red_copy(j, me).start()
+
+    def drain(l, carry):
+        for s in range(PIECES):
+            for d in range(2):
+                for h in range(1, half + 1):
+                    if h < half or s % 2 == d:
+                        x_copy(l, d, h, s, 1).wait_send()
+
+        @pl.when(col < cols - 1)
+        def _():
+            for d, h, s in everything:
+                b_copy(l, d, h, s).wait_send()
+
+        def drain_tile(t, carry):
+            for d in range(2):
+                for h in range(1, half):
+                    h_copy(l, d, h, t, 1).wait_send()
+
+                @pl.when(t % 2 == d)
+                def _():
+                    h_copy(l, d, half, t, 1).wait_send()
+
+            return carry
+
+        lax.fori_loop(0, TILES, drain_tile, 0)
+        return carry
+
+    lax.fori_loop(0, layers, drain, 0)
+
+    for j in range(1, n):
+        red_copy(j, (me + n - j) % n).wait_recv()
+    total = jnp.sum(red[:, 0:1, :], axis=0)
+    inv = lax.rsqrt(total / depth + epsilon)
+    out_ref[...] = (wide * inv * fgain_ref[...]).astype(jnp.bfloat16)
+    for j in range(1, n):
+        red_copy(j, me).wait_send()
+
+
+def per_device(
+    n,
+    cols,
+    activations,
+    norm_gain,
+    gate_weight,
+    gate_scale,
+    value_weight,
+    value_scale,
+    gate_taps,
+    value_taps,
+    down_weight,
+    down_scale,
+    final_gain,
+):
+    toks, width = activations.shape
+    layers, depth, units = gate_weight.shape
+    taps = gate_taps.shape[1]
+    hidden = down_weight.shape[1]
+    fits = (
+        n % 2 == 0
+        and n >= 4
+        and cols >= 3
+        and toks == 128
+        and taps == 3
+        and width % (16 * PIECES) == 0
+        and units % (16 * TILES) == 0
+        and depth % 128 == 0
+        and hidden % (128 * DOWN_BLOCKS) == 0
+    )
+    if not fits:
+        return plain_device(
+            activations,
+            norm_gain,
+            gate_weight,
+            gate_scale,
+            value_weight,
+            value_scale,
+            gate_taps,
+            value_taps,
+            down_weight,
+            down_scale,
+            final_gain,
+        )
+    par = jnp.concatenate(
+        [gate_scale[:, None], value_scale[:, None], gate_taps, value_taps], axis=1
+    )
+    par = jnp.swapaxes(par, 1, 2)
+    half = n // 2
+    tile = units // TILES
+    kblock = hidden // DOWN_BLOCKS
+    vm = pl.BlockSpec(memory_space=pltpu.VMEM)
+    hbm = pl.BlockSpec(memory_space=pl.ANY)
+    dma = pltpu.SemaphoreType.DMA
+    out = pl.pallas_call(
+        functools.partial(fused_kernel, n, cols),
+        out_shape=jax.ShapeDtypeStruct((width, toks), jnp.bfloat16),
+        in_specs=[vm] * 5 + [hbm] * 3,
+        out_specs=vm,
+        scratch_shapes=[
+            pltpu.VMEM((layers + 1, depth, toks), jnp.bfloat16),
+            pltpu.VMEM((layers, depth, toks), jnp.bfloat16),
+            pltpu.VMEM((depth, 2 * toks), jnp.bfloat16),
+            pltpu.VMEM((layers, hidden, toks), jnp.bfloat16),
+            pltpu.VMEM((GV_SLOTS, tile, depth), jnp.float32),
+            pltpu.VMEM((GV_SLOTS, tile, depth), jnp.float32),
+            pltpu.VMEM((DOWN_SLOTS, width, kblock), jnp.float32),
+            pltpu.VMEM((width, toks), jnp.float32),
+            pltpu.VMEM((1, 2 * toks), jnp.float32),
+            pltpu.VMEM((n, 8, toks), jnp.float32),
+            dma((GV_SLOTS,)),
+            dma((GV_SLOTS,)),
+            dma((DOWN_SLOTS,)),
+            dma((layers, 2, half, PIECES)),
+            dma((layers, 2, half, PIECES)),
+            dma((layers, 2, half + 1, PIECES)),
+            dma((layers, 2, half + 1, PIECES)),
+            dma((layers, 2, half, TILES)),
+            dma((layers, 2, half, TILES)),
+            dma((n,)),
+            dma((n,)),
+        ],
+        compiler_params=pltpu.CompilerParams(
+            collective_id=0, has_side_effects=True, vmem_limit_bytes=66 * 1000 * 1000
+        ),
+    )(
+        activations.T,
+        norm_gain[:, :, None],
+        par,
+        down_scale[:, :, None],
+        final_gain[:, None],
+        jnp.swapaxes(gate_weight, 1, 2),
+        jnp.swapaxes(value_weight, 1, 2),
+        jnp.swapaxes(down_weight, 1, 2),
+    )
+    return out.T
+
+
 def solution(mesh):
     in_specs = (
         P("cb", "ra"),
@@ -100,6 +527,7 @@
         P("ra"),
     )
     out_specs = P("cb", "ra")
+    body = functools.partial(per_device, mesh.shape["ra"], mesh.shape["cb"])
     return jax.shard_map(
-        per_device, mesh=mesh, in_specs=in_specs, out_specs=out_specs, check_vma=False
+        body, mesh=mesh, in_specs=in_specs, out_specs=out_specs, check_vma=False
     )

time: 317 us -> 147 us (0.46)
  waiting for transfers between devices: 133 us -> 0 us
  Pallas kernels: 0 us -> 132 us
  other arithmetic: 85.8 us -> 4.17 us
  matrix products: 48.9 us -> 0 us
  blocking collectives: 19.1 us -> 0 us
  between operations: 13.4 us -> 0.06 us
  starting transfers between devices: 12.6 us -> 0 us
  local copies, waits for them, and re-layouts: 3.63 us -> 11.1 us
    pallas_call x0 -> x1, Pallas kernels: none -> 132 us  [per_device(): pl.pallas_call(functools.partial(fused_kernel, n, cols), out_shape=jax.Sh...]
    all_gather x4 -> x0, waiting for transfers between devices: 132 us -> none  [the longest x2 92.4 us: per_device(): lax.all_gather(hidden, 'ra', axis=1, tiled=True)]
    another operation x3 -> x0, other arithmetic: 74.7 us -> none
    dot_general x6 -> x0, matrix products: 48.9 us -> none  [the longest x2 16.5 us: per_device(): jnp.dot(scaled, gate_weight[layer_idx].astype(jnp.bfloat16), preferred_el...]
    psum x1 -> x0, blocking collectives: 19.1 us -> none  [per_device(): sq_final = lax.psum(jnp.sum(wide_rows * wide_rows, axis=1), 'ra')]
    ppermute x4 -> x0, starting transfers between devices: 12.2 us -> none  [from_behind(): return lax.ppermute(value, axis, pairs)]
    convert_element_type x3 -> x0, other arithmetic: 7.4 us -> none  [the longest x2 6.6 us: per_device(): hidden = (jax.nn.silu(gate_conv) * value_conv).astype(jnp.bfloat16)]
    broadcast_in_dim x0 -> x5, local copies, waits for them, and re-layouts: none -> 6.33 us  [the longest x1 2.79 us: per_device(): norm_gain[:, :, None]]
  transfers between devices with their start and end apart: 8 -> 0, of which waited for: 5 -> 0; matrix products, arithmetic and copies ran while one was open for 29% -> 0% of each run, Pallas kernels for 0% -> 0%
where the time goes in v1:
time: 147 us
  Pallas kernels  132 us (90%)
  local copies, waits for them, and re-layouts  11.1 us (8%)
  other arithmetic  4.17 us (3%)
    pallas_call x1, Pallas kernels, per_device(): pl.pallas_call(functools.partial(fused_kernel, n, cols), out_shape=jax.Sh...  132 us
    unnamed x15, local copies, waits for them, and re-layouts  4.81 us
    transpose x1, other arithmetic, per_device(): par = jnp.swapaxes(par, 1, 2)  4.17 us

profile of v1, /device:TPU:0, one launch (start us, length us, event | category | flops | bytes accessed | tf_op | source)
XLA Modules:
  0.0 147.0 jit_solution(16353056710347595137)
XLA Ops:
  0.0 0.0 copy-start.3
  0.0 0.0 copy-start
  0.0 1.2 copy.29
  1.2 0.0 copy-done.3
  1.2 0.0 copy-start.1
  1.2 0.5 copy.30
  1.7 0.0 copy-done
  1.7 1.6 %copy.31 = f32[2,3,1440]{1,2,0:T(8,128)} copy(f32[2,3,1440]{2,0,1:T(2,128)S(1)} %copy-done) | data formatting | bytes 69120 | tf_op args[6]
  3.3 0.0 copy-done.1
  3.3 1.6 %copy.32 = f32[2,3,1440]{1,2,0:T(8,128)} copy(f32[2,3,1440]{2,0,1:T(2,128)S(1)} %copy-done.1) | data formatting | bytes 69120 | tf_op args[7]
  4.9 0.0 copy-start.2
  4.9 4.2 %maximum_bitcast_fusion.par_ref = f32[2,1440,8]{2,1,0:T(8,128)} fusion(f32[2,3,1440]{1,2,0:T(8,128)} %copy.32, f32[2,3,1440]{1,2,0:T(8,128)} %copy.31, f32[2,1,1440]{1,2,0:T(8,128)S(1)} %copy.30, f32[2,1,1440]{1,2,0:T(8,128)S(1)} %copy.29), kind=kLoop, calls=%fused_computation | loop fusion | flops 69120 | bytes 184320 | tf_op jit(solution)/shard_map/transpose | solution.py:464
  9.1 0.0 copy-done.2
  9.1 0.0 copy-start.4
  9.1 0.0 copy-start.5
  9.1 2.8 %copy.33.gain_ref = f32[2,4224,1]{2,1,0:T(8,128)} copy(f32[2,4224,1]{1,0,2:T(2,128)S(1)} %bitcast.16) | data formatting | bytes 67584 | tf_op jit(solution)/shard_map/broadcast_in_dim | solution.py:504
  11.9 0.0 copy-done.4
  11.9 1.0 copy.34.dscale_ref
  13.0 0.0 copy-done.5
  13.0 0.8 broadcast_in_dim.20.fgain_ref
  13.8 131.7 %shard_map.109 = bf16[528,128]{1,0:T(8,128)(2,1)} custom-call(bf16[528,128]{1,0:T(8,128)(2,1)} %bitcast.15, f32[2,4224,1]{2,1,0:T(8,128)} %copy.33.gain_ref, f32[2,1440,8]{2,1,0:T(8,128)} %maximum_bitcast_fusion.par_ref, f32[2,528,1]{2,1,0:T(8,128)} %copy.34.dscale_ref, f32[528,1]{1,0:T(8,128)} %broadcast_in_dim.20.fgain_ref, f32[2,1440,4224]{2,1,0:T(8,128)} %bitcast.11, ...), custom_call_target="tpu_custom_call" | custom-call | tf_op jit(solution)/shard_map/pallas_call | solution.py:471
  145.5 1.6 %copy.37 = bf16[128,528]{0,1:T(8,128)(2,1)} copy(bf16[128,528]{0,1:T(8,128)(2,1)} %bitcast.14) | data formatting | bytes 270336
Async XLA Ops:
  0.0 1.2 copy-start.3
  0.0 1.7 %copy-start = (f32[2,3,1440]{2,0,1:T(2,128)S(1)}, f32[2,3,1440]{2,0,1:T(2,128)}, u32[]{:S(2)}) copy-start(f32[2,3,1440]{2,0,1:T(2,128)} %param.17) | copy-start | bytes 103684
  1.2 2.1 %copy-start.1 = (f32[2,3,1440]{2,0,1:T(2,128)S(1)}, f32[2,3,1440]{2,0,1:T(2,128)}, u32[]{:S(2)}) copy-start(f32[2,3,1440]{2,0,1:T(2,128)} %param.18) | copy-start | bytes 103684
  4.9 4.2 %copy-start.2 = (f32[2,4224]{1,0:T(2,128)S(1)}, f32[2,4224]{1,0:T(2,128)}, u32[]{:S(2)}) copy-start(f32[2,4224]{1,0:T(2,128)} %param.12) | copy-start | bytes 101380
  9.1 2.8 %copy-start.4 = (f32[2,528]{1,0:T(2,128)S(1)}, f32[2,528]{1,0:T(2,128)}, u32[]{:S(2)}) copy-start(f32[2,528]{1,0:T(2,128)} %param.20) | copy-start | bytes 12676
  9.1 3.8 %copy-start.5 = (f32[528]{0:T(1024)S(1)}, f32[528]{0:T(1024)}, u32[]{:S(2)}) copy-start(f32[528]{0:T(1024)} %param.21) | copy-start | bytes 6340
